TPU v7x, 256 devices: a 4x2x16 block of a 4x16x16 slice. The times are simulated.
256 devices in a mesh: grp: 2 (over y), sp: 32 (over z, core), tp: 4 (over x).
Axes of the slice: x: 4, y: 2, z: 16, core: 2. Of those that a mesh axis runs over, the one named last changes fastest.
The devices are a block of a 4x16x16 slice.
Arguments:
- queries_small: bfloat16 [16384, 1024], P(('grp', 'sp'), 'tp'), parts along dimension 0, may hold values from -6 to 6
- keys_small: bfloat16 [16384, 512], P(('grp', 'sp'), 'tp'), parts along dimension 0, may hold values from -6 to 6
- values_small: bfloat16 [16384, 512], P(('grp', 'sp'), 'tp'), parts along dimension 0, may hold values from -6 to 6
- queries_large: bfloat16 [16384, 1024], P(('grp', 'sp'), 'tp'), parts along dimension 0, may hold values from -6 to 6
- keys_large: bfloat16 [16384, 512], P(('grp', 'sp'), 'tp'), parts along dimension 0, may hold values from -6 to 6
- values_large: bfloat16 [16384, 512], P(('grp', 'sp'), 'tp'), parts along dimension 0, may hold values from -6 to 6
- query_gain_small: float32 [128], P('grp'), parts along dimension 0, may hold values from 1.2 to 12
- key_gain_small: float32 [128], P('grp'), parts along dimension 0, may hold values from 1.2 to 12
- query_gain_large: float32 [256], P('grp'), parts along dimension 0, may hold values from 1.2 to 12
- key_gain_large: float32 [256], P('grp'), parts along dimension 0, may hold values from 1.2 to 12
- residual_in: bfloat16 [16384, 2048], P(('grp', 'sp', 'tp')), parts along dimension 0, may hold values from -1.5 to 1.5
- out_weight_small: bfloat16 [1024, 2048], P('tp'), may hold values from -0.125 to 0.125
- out_weight_large: bfloat16 [1024, 2048], P('tp'), may hold values from -0.125 to 0.125
- norm_gain: float32 [2048], replicated, may hold values from 0.1 to 1.9
- routes: int32 [16384, 2], P(('grp', 'sp', 'tp')), parts along dimension 0, may hold values from 0 to 63, all different within a row; in each aligned block of 64 rows (0 to 63, 64 to 127, ...) at most 4 rows name the same one
- route_scores: float32 [16384, 2], P(('grp', 'sp', 'tp')), parts along dimension 0, may hold values from 0.05 to 1
- expert_gate: bfloat16 [64, 2048, 1024], P('sp', None, 'tp'), may hold values from -0.125 to 0.125
- expert_up: bfloat16 [64, 2048, 1024], P('sp', None, 'tp'), may hold values from -0.125 to 0.125
- expert_down: bfloat16 [64, 1024, 2048], P('sp', 'tp'), may hold values from -0.1875 to 0.1875
Outputs:
- result: bfloat16 [16384, 2048], P(('grp', 'sp', 'tp')), parts along dimension 0
There are 2 independent parts, one for each index of `grp`. A program takes and returns all parts, laid end to end along the dimension named above; an argument that names none is the same for every part. Nothing has to cross between parts.
Inputs may be any that keep to these rules, and one draw needn't show every extreme that they name: `routes`: each token names 2 different experts; within the rows of one device (aligned blocks of 64 tokens) no expert is named more than 4 times, a bound that some block reaches.
All inputs are finite; a program needn't handle non-finite values.
Results may differ from a plain program's by a relative error of at most 0.02.
The roundings to bfloat16 on the way count: a program that leaves them out, or rounds other values in their place, can miss the bound.
Values may be sent and summed in bfloat16 or wider, within the bound.
A program may use at most 128 MiB of HBM per device.

v0:
```python
import jax
import jax.numpy as jnp
from jax import lax
from jax.sharding import PartitionSpec as P

HS_SMALL = 64
HS_LARGE = 128
GRID_W = 64
theta_base = 10000.0
norm_eps = 1e-06
block_target = 1280


def sent_together(arrays, axis, dim, along):
    ends, at = ([], 0)
    for a in arrays[:-1]:
        at += a.shape[along]
        ends.append(at)
    both = jnp.concatenate(arrays, axis=along)
    return tuple(jnp.split(lax.all_gather(both, axis, axis=dim, tiled=True), ends, axis=along))


def in_blocks(shard, dim, size):
    before, after = (shard.shape[:dim], shard.shape[dim + 1 :])
    return jnp.moveaxis(shard.reshape(*before, size, -1, *after), dim, 0)


def sent_and_summed(shard, axis, dim):
    blocks = in_blocks(shard, dim, lax.axis_size(axis))
    arrived = lax.all_to_all(blocks, axis, split_axis=0, concat_axis=0, tiled=True)
    return arrived.astype(jnp.float32).sum(axis=0)


def grid_tables(offset, length, head_size):
    places = offset + jnp.arange(length, dtype=jnp.int32)
    grid_rows = (places // GRID_W).astype(jnp.float32)
    grid_cols = (places % GRID_W).astype(jnp.float32)
    rates = jnp.power(
        theta_base, -2.0 * jnp.arange(head_size // 4, dtype=jnp.float32) / (head_size // 2)
    )
    row_angles = grid_rows[:, None, None] * rates
    col_angles = grid_cols[:, None, None] * rates
    return (jnp.cos(row_angles), jnp.sin(row_angles), jnp.cos(col_angles), jnp.sin(col_angles))


def half_turn(segment, cosine, sine_part):
    half_size = segment.shape[-1] // 2
    leading = segment[..., :half_size]
    trailing = segment[..., half_size:]
    return jnp.concatenate(
        [leading * cosine - trailing * sine_part, trailing * cosine + leading * sine_part], axis=-1
    )


def grid_turn(vectors, tables):
    row_cos, row_sin, col_cos, col_sin = tables
    half_size = vectors.shape[-1] // 2
    return jnp.concatenate(
        [
            half_turn(vectors[..., :half_size], row_cos, row_sin),
            half_turn(vectors[..., half_size:], col_cos, col_sin),
        ],
        axis=-1,
    )


def normed_turn(raw_rows, gain, tables):
    widened = raw_rows.astype(jnp.float32)
    scaled = (
        widened * lax.rsqrt(jnp.mean(widened * widened, axis=-1, keepdims=True) + norm_eps) * gain
    )
    return grid_turn(scaled, tables).astype(jnp.bfloat16)


def block_rows(row_count, shard_rows):
    shards = row_count // shard_rows
    chosen = 1
    for factor in range(1, max(1, block_target // shard_rows) + 1):
        if shards % factor == 0:
            chosen = factor
    return chosen * shard_rows


def attend_block(state, queries, key_rows, value_rows):
    largest, weight_sum, accumulated = state
    head_size = queries.shape[-1]
    kv_local = queries.shape[1]
    key_heads = key_rows.reshape(key_rows.shape[0], kv_local, head_size)
    value_heads = value_rows.reshape(value_rows.shape[0], kv_local, head_size)
    scores = jnp.einsum(
        "qgrd,kgd->qgrk", queries, key_heads, preferred_element_type=jnp.float32
    ) * head_size ** (-0.5)
    peak_score = jnp.maximum(largest, jnp.max(scores, axis=-1))
    shrink = jnp.exp(largest - peak_score)
    weights = jnp.exp(scores - peak_score[..., None])
    weight_sum = weight_sum * shrink + jnp.sum(weights, axis=-1)
    accumulated = accumulated * shrink[..., None] + jnp.einsum(
        "qgrk,kgd->qgrd",
        weights.astype(jnp.bfloat16),
        value_heads,
        preferred_element_type=jnp.float32,
    )
    return (peak_score, weight_sum, accumulated)


def attend_rows(state, queries, key_rows, value_rows):
    row_count = key_rows.shape[0]
    step_rows = block_rows(row_count, queries.shape[0])

    def one_block(block_index, carried):
        offset = block_index * step_rows
        return attend_block(
            carried,
            queries,
            lax.dynamic_slice_in_dim(key_rows, offset, step_rows, 0),
            lax.dynamic_slice_in_dim(value_rows, offset, step_rows, 0),
        )

    return lax.fori_loop(0, row_count // step_rows, one_block, state)


def empty_state(queries):
    state_shape = queries.shape[:3]
    return (
        jnp.full(state_shape, -1e30, jnp.float32),
        jnp.zeros(state_shape, jnp.float32),
        jnp.zeros(queries.shape, jnp.float32),
    )


def finish(state):
    largest, weight_sum, accumulated = state
    merged = accumulated / weight_sum[..., None]
    return merged.reshape(merged.shape[0], -1).astype(jnp.bfloat16)


def on_device(
    queries_small,
    keys_small,
    values_small,
    queries_large,
    keys_large,
    values_large,
    query_gain_small,
    key_gain_small,
    query_gain_large,
    key_gain_large,
    residual_in,
    out_weight_small,
    out_weight_large,
    norm_gain,
    routes,
    route_scores,
    expert_gate,
    expert_up,
    expert_down,
):
    token_rows = queries_small.shape[0]
    offset = lax.axis_index("sp") * token_rows
    tables_small = grid_tables(offset, token_rows, HS_SMALL)
    tables_large = grid_tables(offset, token_rows, HS_LARGE)
    kv_small = keys_small.shape[1] // HS_SMALL
    kv_large = keys_large.shape[1] // HS_LARGE
    asked_small = normed_turn(
        queries_small.reshape(token_rows, -1, HS_SMALL), query_gain_small, tables_small
    ).reshape(token_rows, kv_small, -1, HS_SMALL)
    asked_large = normed_turn(
        queries_large.reshape(token_rows, -1, HS_LARGE), query_gain_large, tables_large
    ).reshape(token_rows, kv_large, -1, HS_LARGE)
    turned_small = normed_turn(
        keys_small.reshape(token_rows, kv_small, HS_SMALL), key_gain_small, tables_small
    ).reshape(token_rows, -1)
    turned_large = normed_turn(
        keys_large.reshape(token_rows, kv_large, HS_LARGE), key_gain_large, tables_large
    ).reshape(token_rows, -1)
    key_small, value_small, key_large, value_large = sent_together(
        (turned_small, values_small, turned_large, values_large), "sp", 0, 1
    )
    state_small = attend_rows(empty_state(asked_small), asked_small, key_small, value_small)
    state_large = attend_rows(empty_state(asked_large), asked_large, key_large, value_large)
    heard_small = finish(state_small)
    heard_large = finish(state_large)
    projected = sent_and_summed(
        (
            jnp.dot(heard_small, out_weight_small, preferred_element_type=jnp.float32)
            + jnp.dot(heard_large, out_weight_large, preferred_element_type=jnp.float32)
        ).astype(jnp.bfloat16),
        "tp",
        0,
    )
    attended = (residual_in.astype(jnp.float32) + projected).astype(jnp.bfloat16)
    widened = attended.astype(jnp.float32)
    normed = (
        widened
        * lax.rsqrt(jnp.mean(widened * widened, axis=-1, keepdims=True) + norm_eps)
        * norm_gain
    ).astype(jnp.bfloat16)
    local_rows = routes.shape[0]
    top_count = routes.shape[1]
    sp_count = lax.axis_size("sp")
    local_experts = expert_gate.shape[0]
    expert_count = local_experts * sp_count
    capacity = max(2, (2 * top_count * local_rows + expert_count - 1) // expert_count)
    flat_routes = routes.reshape(-1)
    member = (flat_routes[:, None] == jnp.arange(expert_count, dtype=jnp.int32)[None, :]).astype(
        jnp.int32
    )
    ranks = jnp.sum((jnp.cumsum(member, axis=0) - member) * member, axis=1)
    slots = flat_routes * capacity + ranks
    picker = (
        slots[:, None] == jnp.arange(expert_count * capacity, dtype=jnp.int32)[None, :]
    ).astype(jnp.bfloat16)
    placer = jnp.sum(picker.reshape(local_rows, top_count, -1), axis=1)
    outgoing = jnp.einsum("ts,td->sd", placer, normed, preferred_element_type=jnp.float32).astype(
        jnp.bfloat16
    )
    outgoing = outgoing.reshape(sp_count, local_experts, capacity, -1)
    everyone = lax.all_gather(
        lax.all_to_all(outgoing, "sp", split_axis=0, concat_axis=0, tiled=True),
        "tp",
        axis=0,
        tiled=True,
    )
    gate_out = jnp.einsum(
        "secd,edf->secf", everyone, expert_gate, preferred_element_type=jnp.float32
    )
    up_out = jnp.einsum("secd,edf->secf", everyone, expert_up, preferred_element_type=jnp.float32)
    active = (jax.nn.silu(gate_out) * up_out).astype(jnp.bfloat16)
    summed = lax.psum_scatter(
        jnp.einsum(
            "secf,efd->secd", active, expert_down, preferred_element_type=jnp.float32
        ).astype(jnp.bfloat16),
        "tp",
        scatter_dimension=0,
        tiled=True,
    )
    returned = lax.all_to_all(summed, "sp", split_axis=0, concat_axis=0, tiled=True)
    back_rows = returned.reshape(expert_count * capacity, -1)
    chosen_rows = jnp.dot(picker, back_rows, preferred_element_type=jnp.float32).reshape(
        local_rows, top_count, -1
    )
    shares = route_scores / jnp.sum(route_scores, axis=1, keepdims=True)
    mixed = jnp.sum(chosen_rows * shares[:, :, None], axis=1)
    return (attended.astype(jnp.float32) + mixed).astype(jnp.bfloat16)


def solution(mesh):
    in_specs = (
        P(("grp", "sp"), "tp"),
        P(("grp", "sp"), "tp"),
        P(("grp", "sp"), "tp"),
        P(("grp", "sp"), "tp"),
        P(("grp", "sp"), "tp"),
        P(("grp", "sp"), "tp"),
        P("grp"),
        P("grp"),
        P("grp"),
        P("grp"),
        P(("grp", "sp", "tp"), None),
        P("tp", None),
        P("tp", None),
        P(),
        P(("grp", "sp", "tp"), None),
        P(("grp", "sp", "tp"), None),
        P("sp", None, "tp"),
        P("sp", None, "tp"),
        P("sp", "tp", None),
    )
    out_specs = P(("grp", "sp", "tp"), None)
    return jax.shard_map(
        on_device, mesh=mesh, in_specs=in_specs, out_specs=out_specs, check_vma=False
    )
```

profile of v0, /device:TPU:33, one launch (start us, length us, event | category | flops | bytes accessed | tf_op | source)
XLA Modules:
  0.0 520.4 jit_solution(17485946820454856762)
XLA Ops:
  6.6 1.1 copy.84
  8.8 0.9 copy.86
  12.3 0.9 copy.87
  15.2 107.8 %all-gather.3.cloned.1.call-done = bf16[8192,512]{0,1:T(8,128)(2,1)} async-done(((bf16[256,512]{0,1:T(8,128)(2,1)}), bf16[8192,512]{0,1:T(8,128)(2,1)}) %all-gather.3.cloned.1.call-update) | async-done | bytes 8388624 | tf_op jit(solution)/shard_map/all_gather | solution.py:20
  123.0 6.0 %fusion.100 = (bf16[8192,128]{0,1:T(8,128)(2,1)}, bf16[8192,128]{0,1:T(8,128)(2,1)}, bf16[8192,128]{0,1:T(8,128)(2,1)}, bf16[8192,128]{0,1:T(8,128)(2,1)}) fusion(bf16[8192,512]{0,1:T(8,128)(2,1)} %all-gather.3.cloned.1.call-done), kind=kLoop, calls=%fused_computation.172 | loop fusion | bytes 16777216 | tf_op jit(solution)/shard_map/split | solution.py:20
  129.0 44.6 %while.37 = (s32[]{:T(128)}, f32[256,1,2]{0,2,1:T(2,128)S(1)}, f32[256,1,2]{0,2,1:T(2,128)S(1)}, f32[256,1,2,128]{0,3,2,1:T(8,128)S(1)}, bf16[8192,128]{0,1:T(8,...) while((s32[]{:T(128)}, f32[256,1,2]{0,2,1:T(2,128)S(1)}, ...), condition=%wide.region_11.12_spmd.clone, body=%wide.region_8.11_spmd.clone.sunk | while | flops 272829440 | bytes 15892683 | solution.py:119
  129.0 2.8 bitcast_reduce_fusion.5
  131.8 2.4 fusion.138
  134.6 2.8 bitcast_reduce_fusion.5
  137.3 2.4 fusion.138
  140.1 2.8 bitcast_reduce_fusion.5
  142.9 2.4 fusion.138
  145.7 2.8 bitcast_reduce_fusion.5
  148.5 2.4 fusion.138
  151.3 2.8 bitcast_reduce_fusion.5
  154.1 2.4 fusion.138
  156.9 2.8 bitcast_reduce_fusion.5
  159.6 2.4 fusion.138
  162.4 2.8 bitcast_reduce_fusion.5
  165.2 2.4 fusion.138
  168.0 2.8 bitcast_reduce_fusion.5
  170.8 2.4 fusion.138
  173.6 64.9 %while.36 = (s32[]{:T(128)}, f32[256,2,2]{0,2,1:T(2,128)S(1)}, f32[256,2,2]{0,2,1:T(2,128)S(1)}, f32[256,2,2,64]{0,3,2,1:T(8,128)S(1)}, bf16[8192,128]{0,1:T(8,1...) while((s32[]{:T(128)}, f32[256,2,2]{0,2,1:T(2,128)S(1)}, ...), condition=%wide.region_6.7_spmd.clone, body=%wide.region_3.6_spmd.clone.sunk | while | flops 277025792 | bytes 31654084 | solution.py:119
  173.6 1.1 constant_dynamic-slice_fusion.3
  174.7 2.7 bitcast_reduce_fusion.4
  177.4 3.0 fusion.131
  181.7 1.1 constant_dynamic-slice_fusion.3
  182.8 2.7 bitcast_reduce_fusion.4
  185.5 3.0 fusion.131
  189.8 1.1 constant_dynamic-slice_fusion.3
  190.9 2.7 bitcast_reduce_fusion.4
  193.6 3.0 fusion.131
  197.9 1.1 constant_dynamic-slice_fusion.3
  199.0 2.7 bitcast_reduce_fusion.4
  201.7 3.0 fusion.131
  206.1 1.1 constant_dynamic-slice_fusion.3
  207.1 2.7 bitcast_reduce_fusion.4
  209.8 3.0 fusion.131
  214.2 1.1 constant_dynamic-slice_fusion.3
  215.2 2.7 bitcast_reduce_fusion.4
  217.9 3.0 fusion.131
  222.3 1.1 constant_dynamic-slice_fusion.3
  223.3 2.7 bitcast_reduce_fusion.4
  226.0 3.0 fusion.131
  230.4 1.1 constant_dynamic-slice_fusion.3
  231.5 2.7 bitcast_reduce_fusion.4
  234.1 3.0 fusion.131
  238.6 1.8 fusion.101
  240.3 1.5 fusion.32
  241.8 4.1 all-to-all-start
  246.9 13.6 %all-to-all-done = bf16[4,64,2048]{2,1,0:T(8,128)(2,1)S(1)} async-done(((bf16[4,64,2048]{2,1,0:T(8,128)(2,1)}), bf16[4,64,2048]{2,1,0:T(8,128)(2,1)S(1)}, u32[]{:S(2)}, u32[]{:S(2)}) %all-to-all-start) | async-done | bytes 1048608 | tf_op jit(solution)/shard_map/all_to_all | solution.py:30
  260.7 1.1 fusion.53
  262.4 1.2 reshape.651
  263.6 64.4 %all_to_all.15 = bf16[32,2,4,2048]{3,2,1,0:T(4,128)(2,1)S(1)} all-to-all(bf16[32,2,4,2048]{3,2,1,0:T(4,128)(2,1)} %reshape.651), channel_id=1, replica_groups=mesh['grp'=2,'sp'=32,'tp'=4] {'sp'}, dimensions={0} | all-to-all | bytes 2097152 | tf_op jit(solution)/shard_map/all_to_all | solution.py:219
  328.0 1.6 copy.94
  329.9 43.8 %all-gather.5.cloned.1.call-done = bf16[128,2,4,2048]{3,0,2,1:T(8,128)(2,1)} async-done(((bf16[32,2,4,2048]{3,0,2,1:T(8,128)(2,1)}), bf16[128,2,4,2048]{3,0,2,1:T(8,128)(2,1)}) %all-gather.5.cloned.1.call-update) | async-done | bytes 4194320 | tf_op jit(solution)/shard_map/all_gather | solution.py:218
  373.7 4.1 fusion.38
  377.8 7.3 %convert_bitcast_fusion = bf16[128,2,4,2048]{3,0,2,1:T(8,128)(2,1)} fusion(bf16[2,256,2048]{2,1,0:T(8,128)(2,1)S(1)} %copy-done, bf16[128,2,4,2048]{3,0,2,1:T(8,128)(2,1)} %all-gather.5.cloned.1.call-done, bf16[2,2048,256]{2,1,0:T(8,128)(2,1)} %param.40, f32[128,2,4,256]{3,0,2,1:T(8,128)S(1)} %fusion.38), kind=kOutput, calls=%fused_computation.43 | convolution fusion | flops 2151153664 | bytes 13631488 | tf_op jit(solution)/shard_map/secf,efd->secd/dot_general | solution.py:230
  385.2 53.5 %reduce-scatter.2.cloned.1.call-done = bf16[32,2,4,2048]{3,0,2,1:T(8,128)(2,1)} async-done(((bf16[128,2,4,2048]{3,0,2,1:T(8,128)(2,1)}), bf16[32,2,4,2048]{3,0,2,1:T(8,128)(2,1)}) %reduce-scatter.2.cloned.1.call-update) | async-done | bytes 1048592 | tf_op jit(solution)/shard_map/reduce_scatter | solution.py:229
  438.7 3.1 copy.95
  441.8 13.2 %all-to-all-start.2 = ((bf16[32,2,4,2048]{3,2,1,0:T(4,128)(2,1)}), bf16[32,2,4,2048]{3,2,1,0:T(4,128)(2,1)S(1)}, u32[]{:S(2)}, u32[]{:S(2)}) async-start(bf16[32,2,4,2048]{3,2,1,0:T(4,128)(2,1)} %copy.95), calls=%async_computation.3 | async-start | bytes 2097152 | tf_op jit(solution)/shard_map/all_to_all | solution.py:237
  455.0 55.4 %all-to-all-done.2 = bf16[32,2,4,2048]{3,2,1,0:T(4,128)(2,1)S(1)} async-done(((bf16[32,2,4,2048]{3,2,1,0:T(4,128)(2,1)}), bf16[32,2,4,2048]{3,2,1,0:T(4,128)(2,1)S(1)}, u32[]{:S(2)}, u32[]{:S(2)}) %all-to-all-start.2) | async-done | bytes 1048608 | tf_op jit(solution)/shard_map/all_to_all | solution.py:237
  510.4 1.1 reshape.667
  511.5 1.6 fusion.50
  (179 shorter events, 21.6 us)
Async XLA Ops:
  6.5 371.2 %copy-start = (bf16[2,256,2048]{2,1,0:T(8,128)(2,1)S(1)}, bf16[2,256,2048]{2,1,0:T(8,128)(2,1)}, u32[]{:S(2)}) copy-start(bf16[2,256,2048]{2,1,0:T(8,128)(2,1)} %param.41) | copy-start | bytes 6291460
  6.6 7.5 %copy-start.5 = (bf16[256,256]{1,0:T(8,128)(2,1)S(1)}, bf16[256,256]{1,0:T(8,128)(2,1)}, u32[]{:S(2)}) copy-start(bf16[256,256]{1,0:T(8,128)(2,1)} %param.26) | copy-start | bytes 393220
  6.6 8.0 %copy-start.10 = (f32[128]{0:T(128)S(1)}, f32[128]{0:T(128)}, u32[]{:S(2)}) copy-start(f32[128]{0:T(128)} %param.31) | copy-start | bytes 1540
  6.6 116.5 %all-gather.3.cloned.1.call-start = ((), (), s32[]{:S(2)}) async-start(), calls=%async_computation.4 | async-start | bytes 8650752 | tf_op jit(solution)/shard_map/all_gather | solution.py:20
  8.5 6.4 %copy-start.6 = (bf16[256,256]{1,0:T(8,128)(2,1)S(1)}, bf16[256,256]{1,0:T(8,128)(2,1)}, u32[]{:S(2)}) copy-start(bf16[256,256]{1,0:T(8,128)(2,1)} %param.23) | copy-start | bytes 393220
  8.7 6.3 %copy-start.11 = (f32[64]{0:T(128)S(1)}, f32[64]{0:T(128)}, u32[]{:S(2)}) copy-start(f32[64]{0:T(128)} %param.29) | copy-start | bytes 772
  13.2 0.7 copy-start.4
  131.7 2.4 copy-start.2
  137.3 2.4 copy-start.2
  142.9 2.4 copy-start.2
  148.5 2.4 copy-start.2
  154.1 2.4 copy-start.2
  159.6 2.4 copy-start.2
  165.2 2.4 copy-start.2
  170.8 2.4 copy-start.2
  177.4 3.4 copy-start.1
  185.5 3.4 copy-start.1
  193.6 3.4 copy-start.1
  201.7 3.4 copy-start.1
  209.8 3.4 copy-start.1
  217.9 3.4 copy-start.1
  226.0 3.4 copy-start.1
  234.1 3.4 copy-start.1
  238.5 1.8 copy-start.3
  241.8 4.1 copy-start.8
  241.8 20.1 %copy-start.7 = (f32[2048]{0:T(1024)S(1)}, f32[2048]{0:T(1024)}, u32[]{:S(2)}) copy-start(f32[2048]{0:T(1024)} %param.36) | copy-start | bytes 24580
  241.8 18.8 %all-to-all-start = ((bf16[4,64,2048]{2,1,0:T(8,128)(2,1)}), bf16[4,64,2048]{2,1,0:T(8,128)(2,1)S(1)}, u32[]{:S(2)}, u32[]{:S(2)}) async-start(bf16[4,64,2048]{2,1,0:T(8,128)(2,1)} %bitcast.205), calls=%async_computation | async-start | bytes 2097152 | tf_op jit(solution)/shard_map/all_to_all | solution.py:30
  245.9 127.8 %all-gather.5.cloned.1.call-start = ((), (), s32[]{:S(2)}) async-start(), calls=%async_computation.5 | async-start | bytes 5242880 | tf_op jit(solution)/shard_map/all_gather | solution.py:218
  329.6 109.1 %reduce-scatter.2.cloned.1.call-start = ((), (), s32[]{:S(2)}) async-start(), calls=%async_computation.6 | async-start | bytes 5242880 | tf_op jit(solution)/shard_map/reduce_scatter | solution.py:229
  385.2 69.8 %copy-start.9 = (f32[64,2]{0,1:T(2,128)S(1)}, f32[64,2]{0,1:T(2,128)}, u32[]{:S(2)}) copy-start(f32[64,2]{0,1:T(2,128)} %param.38) | copy-start | bytes 1540
  441.8 68.6 %all-to-all-start.2 = ((bf16[32,2,4,2048]{3,2,1,0:T(4,128)(2,1)}), bf16[32,2,4,2048]{3,2,1,0:T(4,128)(2,1)S(1)}, u32[]{:S(2)}, u32[]{:S(2)}) async-start(bf16[32,2,4,2048]{3,2,1,0:T(4,128)(2,1)} %copy.95), calls=%async_computation.3 | async-start | bytes 2097152 | tf_op jit(solution)/shard_map/all_to_all | solution.py:237
Sparse Core Ops, SparseCore 0:
  14.1 108.8 all-gather.2
  329.7 43.8 all-gather.4
  385.3 53.3 reduce-scatter.1
where the time goes:
time: 522 us; the launch traced here: 520 us
  waiting for transfers between devices  274 us (52%)
  matrix products  86.1 us (16%)
  blocking collectives  64.4 us (12%)
  other arithmetic  33.7 us (6%)
  local copies, waits for them, and re-layouts  30 us (6%)
  starting transfers between devices  17.5 us (3%)
  between operations  13.6 us (3%)
    all_gather x1, waiting for transfers between devices, sent_together(): lax.all_gather(both, axis, axis=dim, tiled=True)  108 us
    all_to_all x1, blocking collectives, on_device(): lax.all_to_all(outgoing, 'sp', split_axis=0, concat_axis=0, tiled=True)  64.4 us
    all_to_all x1, waiting for transfers between devices, on_device(): lax.all_to_all(summed, 'sp', split_axis=0, concat_axis=0, tiled=True)  55.4 us
    reduce_scatter x1, waiting for transfers between devices, on_device(): lax.psum_scatter(jnp.einsum('secf,efd->secd', active, expert_down, prefer...  53.5 us
    all_gather x1, waiting for transfers between devices, on_device(): lax.all_gather(lax.all_to_all(outgoing, 'sp', split_axis=0, concat_axis=0...  43.8 us
    dot_general x16, matrix products, attend_block(): jnp.einsum('qgrd,kgd->qgrk', queries, key_heads, preferred_element_type=j...  43.6 us
    reduce_sum x16, other arithmetic, attend_block(): weight_sum = weight_sum * shrink + jnp.sum(weights, axis=-1)  27.2 us
    dot_general x16, matrix products, attend_block(): jnp.einsum('qgrk,kgd->qgrd', weights.astype(jnp.bfloat16), value_heads, p...  25.8 us
  transfers between devices with their start and end apart: 5, of which 5 were waited for; matrix products, arithmetic and copies ran while one was open for 0% of the time, Pallas kernels for 0%

commit v1 on v0

--- a/solution.py
+++ b/solution.py
@@ -9,6 +9,23 @@
 theta_base = 10000.0
 norm_eps = 1e-06
 block_target = 1280
+
+
+def laid_out(parts, dim):
+    dims = list(parts.shape[1:])
+    dims[dim] *= parts.shape[0]
+    return jnp.moveaxis(parts, 0, dim).reshape(dims)
+
+
+def collected_by_bits(x, axis):
+    size, position = (lax.axis_size(axis), lax.axis_index(axis))
+    parts, apart = (x[None], 1)
+    while apart < size:
+        other = lax.ppermute(parts, axis, [(i, i ^ apart) for i in range(size)])
+        low = position & apart == 0
+        parts = jnp.concatenate([jnp.where(low, parts, other), jnp.where(low, other, parts)])
+        apart *= 2
+    return parts
 
 
 def sent_together(arrays, axis, dim, along):
@@ -215,12 +232,8 @@
         jnp.bfloat16
     )
     outgoing = outgoing.reshape(sp_count, local_experts, capacity, -1)
-    everyone = lax.all_gather(
-        lax.all_to_all(outgoing, "sp", split_axis=0, concat_axis=0, tiled=True),
-        "tp",
-        axis=0,
-        tiled=True,
-    )
+    x = lax.all_to_all(outgoing, "sp", split_axis=0, concat_axis=0, tiled=True)
+    everyone = laid_out(collected_by_bits(x, "tp"), 0)
     gate_out = jnp.einsum(
         "secd,edf->secf", everyone, expert_gate, preferred_element_type=jnp.float32
     )

time: 522 us -> 552 us (1.057)
  waiting for transfers between devices: 274 us -> 291 us
  other arithmetic: 33.7 us -> 45.5 us
    ppermute x0 -> x2, waiting for transfers between devices: none -> 70 us  [collected_by_bits(): other = lax.ppermute(parts, axis, [(i, i ^ apart) for i in range(size)])]
    all_gather x1 -> x0, waiting for transfers between devices: 43.8 us -> none  [on_device(): lax.all_gather(lax.all_to_all(outgoing, 'sp', split_axis=0, concat_axis=0...]
    reduce_scatter x1, waiting for transfers between devices: 53.5 us -> 44.3 us  [on_device(): lax.psum_scatter(jnp.einsum('secf,efd->secd', active, expert_down, prefer...]
    select_n x0 -> x2, other arithmetic: none -> 6.29 us  [collected_by_bits(): jnp.where(low, parts, other)]
  transfers between devices with their start and end apart: 5 -> 6, of which waited for: 5 -> 6; matrix products, arithmetic and copies ran while one was open for 0% -> 0% of each run, Pallas kernels for 0% -> 0%
where the time goes in v1:
time: 552 us; the launch traced here: 551 us
  waiting for transfers between devices  291 us (53%)
  matrix products  83.2 us (15%)
  blocking collectives  64.4 us (12%)
  other arithmetic  45.5 us (8%)
  local copies, waits for them, and re-layouts  33.5 us (6%)
  starting transfers between devices  18.4 us (3%)
  between operations  13.9 us (3%)
    all_gather x1, waiting for transfers between devices, sent_together(): lax.all_gather(both, axis, axis=dim, tiled=True)  108 us
    ppermute x2, waiting for transfers between devices, collected_by_bits(): other = lax.ppermute(parts, axis, [(i, i ^ apart) for i in range(size)])  70 us
    all_to_all x1, blocking collectives, on_device(): x = lax.all_to_all(outgoing, 'sp', split_axis=0, concat_axis=0, tiled=True)  64.4 us
    all_to_all x1, waiting for transfers between devices, on_device(): lax.all_to_all(summed, 'sp', split_axis=0, concat_axis=0, tiled=True)  55.4 us
    reduce_scatter x1, waiting for transfers between devices, on_device(): lax.psum_scatter(jnp.einsum('secf,efd->secd', active, expert_down, prefer...  44.3 us
    dot_general x16, matrix products, attend_block(): jnp.einsum('qgrd,kgd->qgrk', queries, key_heads, preferred_element_type=j...  43.6 us
    reduce_sum x16, other arithmetic, attend_block(): weight_sum = weight_sum * shrink + jnp.sum(weights, axis=-1)  27.2 us
    dot_general x16, matrix products, attend_block(): jnp.einsum('qgrk,kgd->qgrd', weights.astype(jnp.bfloat16), value_heads, p...  25.8 us
  transfers between devices with their start and end apart: 6, of which 6 were waited for; matrix products, arithmetic and copies ran while one was open for 0% of the time, Pallas kernels for 0%

profile of v1, /device:TPU:33, one launch (start us, length us, event | category | flops | bytes accessed | tf_op | source)
XLA Modules:
  0.0 550.9 jit_solution(5809113418615723452)
XLA Ops:
  6.6 1.1 copy.84
  15.2 107.8 %all-gather.2.cloned.1.call-done = bf16[8192,512]{0,1:T(8,128)(2,1)} async-done(((bf16[256,512]{0,1:T(8,128)(2,1)}), bf16[8192,512]{0,1:T(8,128)(2,1)}) %all-gather.2.cloned.1.call-update) | async-done | bytes 8388624 | tf_op jit(solution)/shard_map/all_gather | solution.py:37
  123.0 6.0 %fusion.100 = (bf16[8192,128]{0,1:T(8,128)(2,1)}, bf16[8192,128]{0,1:T(8,128)(2,1)}, bf16[8192,128]{0,1:T(8,128)(2,1)}, bf16[8192,128]{0,1:T(8,128)(2,1)}) fusion(bf16[8192,512]{0,1:T(8,128)(2,1)} %all-gather.2.cloned.1.call-done), kind=kLoop, calls=%fused_computation.178 | loop fusion | bytes 16777216 | tf_op jit(solution)/shard_map/split | solution.py:37
  129.0 44.6 %while.37 = (s32[]{:T(128)}, f32[256,1,2]{0,2,1:T(2,128)S(1)}, f32[256,1,2]{0,2,1:T(2,128)S(1)}, f32[256,1,2,128]{0,3,2,1:T(8,128)S(1)}, bf16[8192,128]{0,1:T(8,...) while((s32[]{:T(128)}, f32[256,1,2]{0,2,1:T(2,128)S(1)}, ...), condition=%wide.region_11.12_spmd.clone, body=%wide.region_8.11_spmd.clone.sunk | while | flops 272829440 | bytes 15892683 | solution.py:136
  129.0 2.8 bitcast_reduce_fusion.5
  131.8 2.4 fusion.138
  134.6 2.8 bitcast_reduce_fusion.5
  137.3 2.4 fusion.138
  140.1 2.8 bitcast_reduce_fusion.5
  142.9 2.4 fusion.138
  145.7 2.8 bitcast_reduce_fusion.5
  148.5 2.4 fusion.138
  151.3 2.8 bitcast_reduce_fusion.5
  154.1 2.4 fusion.138
  156.9 2.8 bitcast_reduce_fusion.5
  159.6 2.4 fusion.138
  162.4 2.8 bitcast_reduce_fusion.5
  165.2 2.4 fusion.138
  168.0 2.8 bitcast_reduce_fusion.5
  170.8 2.4 fusion.138
  173.6 64.9 %while.36 = (s32[]{:T(128)}, f32[256,2,2]{0,2,1:T(2,128)S(1)}, f32[256,2,2]{0,2,1:T(2,128)S(1)}, f32[256,2,2,64]{0,3,2,1:T(8,128)S(1)}, bf16[8192,128]{0,1:T(8,1...) while((s32[]{:T(128)}, f32[256,2,2]{0,2,1:T(2,128)S(1)}, ...), condition=%wide.region_6.7_spmd.clone, body=%wide.region_3.6_spmd.clone.sunk | while | flops 277025792 | bytes 31654084 | solution.py:136
  173.6 1.1 constant_dynamic-slice_fusion.3
  174.7 2.7 bitcast_reduce_fusion.4
  177.4 3.0 fusion.131
  181.7 1.1 constant_dynamic-slice_fusion.3
  182.8 2.7 bitcast_reduce_fusion.4
  185.5 3.0 fusion.131
  189.8 1.1 constant_dynamic-slice_fusion.3
  190.9 2.7 bitcast_reduce_fusion.4
  193.6 3.0 fusion.131
  197.9 1.1 constant_dynamic-slice_fusion.3
  199.0 2.7 bitcast_reduce_fusion.4
  201.7 3.0 fusion.131
  207.1 2.7 bitcast_reduce_fusion.4
  209.8 3.0 fusion.131
  215.2 2.7 bitcast_reduce_fusion.4
  217.9 3.0 fusion.131
  223.3 2.7 bitcast_reduce_fusion.4
  226.0 3.0 fusion.131
  231.5 2.7 bitcast_reduce_fusion.4
  234.1 3.0 fusion.131
  238.6 1.8 fusion.101
  240.3 1.5 fusion.32
  241.8 4.1 all-to-all-start
  246.9 13.6 %all-to-all-done = bf16[4,64,2048]{2,1,0:T(8,128)(2,1)S(1)} async-done(((bf16[4,64,2048]{2,1,0:T(8,128)(2,1)}), bf16[4,64,2048]{2,1,0:T(8,128)(2,1)S(1)}, u32[]{:S(2)}, u32[]{:S(2)}) %all-to-all-start) | async-done | bytes 1048608 | tf_op jit(solution)/shard_map/all_to_all | solution.py:47
  260.7 1.1 fusion.53
  262.4 1.2 reshape.654
  263.6 64.4 %all_to_all.15 = bf16[32,2,4,2048]{3,2,1,0:T(4,128)(2,1)S(1)} all-to-all(bf16[32,2,4,2048]{3,2,1,0:T(4,128)(2,1)} %reshape.654), channel_id=1, replica_groups=mesh['grp'=2,'sp'=32,'tp'=4] {'sp'}, dimensions={0} | all-to-all | bytes 2097152 | tf_op jit(solution)/shard_map/all_to_all | solution.py:235
  329.0 23.3 %collective-permute-done = bf16[1,32,2,4,2048]{4,3,2,1,0:T(4,128)(2,1)} collective-permute-done((bf16[1,32,2,4,2048]{4,3,2,1,0:T(4,128)(2,1)S(1)}, bf16[1,32,2,4,2048]{4,3,2,1,0:T(4,128)(2,1)}, u32[]{:S(2)}, u32[]{:S(2)}) %collective-permute-start) | collective-permute-done | bytes 1048608 | tf_op jit(solution)/shard_map/ppermute | solution.py:24
  352.3 2.4 broadcast_select_fusion.5
  354.7 2.8 pad_maximum_fusion.1
  358.4 46.7 %collective-permute-done.1 = bf16[2,32,2,4,2048]{4,3,2,1,0:T(4,128)(2,1)} collective-permute-done((bf16[2,32,2,4,2048]{4,3,2,1,0:T(4,128)(2,1)}, bf16[2,32,2,4,2048]{4,3,2,1,0:T(4,128)(2,1)}, u32[]{:S(2)}, u32[]{:S(2)}) %collective-permute-start.1) | collective-permute-done | bytes 2097184 | tf_op jit(solution)/shard_map/ppermute | solution.py:24
  405.2 3.9 broadcast_select_fusion.3
  409.1 2.7 pad_maximum_fusion
  411.8 2.3 copy.94
  414.1 2.0 copy-done.5
  416.1 1.2 fusion.38
  417.3 7.3 %convert_bitcast_fusion = bf16[128,2,4,2048]{3,0,2,1:T(8,128)(2,1)} fusion(bf16[2,256,2048]{2,1,0:T(8,128)(2,1)S(1)} %copy-done, bf16[128,2,4,2048]{3,0,2,1:T(8,128)(2,1)} %bitcast.211, bf16[2,2048,256]{2,1,0:T(8,128)(2,1)} %param.40, f32[128,2,4,256]{3,0,2,1:T(8,128)S(1)} %fusion.38), kind=kOutput, calls=%fused_computation.44 | convolution fusion | flops 2151153664 | bytes 13631488 | tf_op jit(solution)/shard_map/secf,efd->secd/dot_general | solution.py:243
  424.7 44.3 %reduce-scatter.2.cloned.1.call-done = bf16[32,2,4,2048]{3,0,2,1:T(8,128)(2,1)} async-done(((bf16[128,2,4,2048]{3,0,2,1:T(8,128)(2,1)}), bf16[32,2,4,2048]{3,0,2,1:T(8,128)(2,1)}) %reduce-scatter.2.cloned.1.call-update) | async-done | bytes 1048592 | tf_op jit(solution)/shard_map/reduce_scatter | solution.py:242
  468.9 3.0 copy.95
  471.9 13.1 %all-to-all-start.2 = ((bf16[32,2,4,2048]{3,2,1,0:T(4,128)(2,1)}), bf16[32,2,4,2048]{3,2,1,0:T(4,128)(2,1)S(1)}, u32[]{:S(2)}, u32[]{:S(2)}) async-start(bf16[32,2,4,2048]{3,2,1,0:T(4,128)(2,1)} %copy.95), calls=%async_computation.3 | async-start | bytes 2097152 | tf_op jit(solution)/shard_map/all_to_all | solution.py:250
  485.1 55.4 %all-to-all-done.2 = bf16[32,2,4,2048]{3,2,1,0:T(4,128)(2,1)S(1)} async-done(((bf16[32,2,4,2048]{3,2,1,0:T(4,128)(2,1)}), bf16[32,2,4,2048]{3,2,1,0:T(4,128)(2,1)S(1)}, u32[]{:S(2)}, u32[]{:S(2)}) %all-to-all-start.2) | async-done | bytes 1048608 | tf_op jit(solution)/shard_map/all_to_all | solution.py:250
  540.6 1.1 reshape.671
  541.7 1.6 fusion.50
  (192 shorter events, 29.4 us)
Async XLA Ops:
  6.5 410.8 %copy-start = (bf16[2,256,2048]{2,1,0:T(8,128)(2,1)S(1)}, bf16[2,256,2048]{2,1,0:T(8,128)(2,1)}, u32[]{:S(2)}) copy-start(bf16[2,256,2048]{2,1,0:T(8,128)(2,1)} %param.41) | copy-start | bytes 6291460
  6.6 7.5 %copy-start.8 = (bf16[256,256]{1,0:T(8,128)(2,1)S(1)}, bf16[256,256]{1,0:T(8,128)(2,1)}, u32[]{:S(2)}) copy-start(bf16[256,256]{1,0:T(8,128)(2,1)} %param.26) | copy-start | bytes 393220
  6.6 8.0 %copy-start.13 = (f32[128]{0:T(128)S(1)}, f32[128]{0:T(128)}, u32[]{:S(2)}) copy-start(f32[128]{0:T(128)} %param.31) | copy-start | bytes 1540
  6.6 116.5 %all-gather.2.cloned.1.call-start = ((), (), s32[]{:S(2)}) async-start(), calls=%async_computation.4 | async-start | bytes 8650752 | tf_op jit(solution)/shard_map/all_gather | solution.py:37
  8.5 6.4 %copy-start.9 = (bf16[256,256]{1,0:T(8,128)(2,1)S(1)}, bf16[256,256]{1,0:T(8,128)(2,1)}, u32[]{:S(2)}) copy-start(bf16[256,256]{1,0:T(8,128)(2,1)} %param.23) | copy-start | bytes 393220
  8.7 6.3 %copy-start.14 = (f32[64]{0:T(128)S(1)}, f32[64]{0:T(128)}, u32[]{:S(2)}) copy-start(f32[64]{0:T(128)} %param.29) | copy-start | bytes 772
  13.2 0.7 copy-start.7
  131.7 2.4 copy-start.2
  137.3 2.4 copy-start.2
  142.9 2.4 copy-start.2
  148.5 2.4 copy-start.2
  154.1 2.4 copy-start.2
  159.6 2.4 copy-start.2
  165.2 2.4 copy-start.2
  170.8 2.4 copy-start.2
  177.4 3.4 copy-start.1
  185.5 3.4 copy-start.1
  193.6 3.4 copy-start.1
  201.7 3.4 copy-start.1
  209.8 3.4 copy-start.1
  217.9 3.4 copy-start.1
  226.0 3.4 copy-start.1
  234.1 3.4 copy-start.1
  238.5 1.8 copy-start.6
  241.8 4.1 copy-start.11
  241.8 20.1 %copy-start.10 = (f32[2048]{0:T(1024)S(1)}, f32[2048]{0:T(1024)}, u32[]{:S(2)}) copy-start(f32[2048]{0:T(1024)} %param.36) | copy-start | bytes 24580
  241.8 18.8 %all-to-all-start = ((bf16[4,64,2048]{2,1,0:T(8,128)(2,1)}), bf16[4,64,2048]{2,1,0:T(8,128)(2,1)S(1)}, u32[]{:S(2)}, u32[]{:S(2)}) async-start(bf16[4,64,2048]{2,1,0:T(8,128)(2,1)} %bitcast.212), calls=%async_computation | async-start | bytes 2097152 | tf_op jit(solution)/shard_map/all_to_all | solution.py:47
  245.9 223.0 %reduce-scatter.2.cloned.1.call-start = ((), (), s32[]{:S(2)}) async-start(), calls=%async_computation.5 | async-start | bytes 5242880 | tf_op jit(solution)/shard_map/reduce_scatter | solution.py:242
  328.0 1.0 copy-start.4
  328.0 24.3 %collective-permute-start = (bf16[1,32,2,4,2048]{4,3,2,1,0:T(4,128)(2,1)S(1)}, bf16[1,32,2,4,2048]{4,3,2,1,0:T(4,128)(2,1)}, u32[]{:S(2)}, u32[]{:S(2)}) collective-permute-start(bf16[1,32,2,4,2048]{4,3,2,1,0:T(4,128)(2,1)S(1)} %bitcast.209), channel_id=1, source_target_pairs={{0,1},{1,0},{2,3},{3,2},{4,5},{5,4},{6,7},{7,6},{8,9},{9,8},{10,11... | collective-permute-start | bytes 3145736 | tf_op jit(solution)/shard_map/ppermute | solution.py:24
  354.7 2.8 copy-start.3
  357.5 47.6 %collective-permute-start.1 = (bf16[2,32,2,4,2048]{4,3,2,1,0:T(4,128)(2,1)}, bf16[2,32,2,4,2048]{4,3,2,1,0:T(4,128)(2,1)}, u32[]{:S(2)}, u32[]{:S(2)}) collective-permute-start(bf16[2,32,2,4,2048]{4,3,2,1,0:T(4,128)(2,1)} %pad_maximum_fusion.1), channel_id=1, source_target_pairs={{0,2},{1,3},{2,0},{3,1},{4,6},{5,7},{6,4},{7,5},{8,10},{9,11},{10,... | collective-permute-start | bytes 6291464 | tf_op jit(solution)/shard_map/ppermute | solution.py:24
  411.8 4.3 copy-start.15
  414.1 2.0 copy-start.5
  424.6 60.5 %copy-start.12 = (f32[64,2]{0,1:T(2,128)S(1)}, f32[64,2]{0,1:T(2,128)}, u32[]{:S(2)}) copy-start(f32[64,2]{0,1:T(2,128)} %param.38) | copy-start | bytes 1540
  471.9 68.6 %all-to-all-start.2 = ((bf16[32,2,4,2048]{3,2,1,0:T(4,128)(2,1)}), bf16[32,2,4,2048]{3,2,1,0:T(4,128)(2,1)S(1)}, u32[]{:S(2)}, u32[]{:S(2)}) async-start(bf16[32,2,4,2048]{3,2,1,0:T(4,128)(2,1)} %copy.95), calls=%async_computation.3 | async-start | bytes 2097152 | tf_op jit(solution)/shard_map/all_to_all | solution.py:250
Sparse Core Ops, SparseCore 0:
  14.1 108.8 all-gather.1
  424.8 44.1 reduce-scatter.1
